TPU v7x, 32 devices: a whole 2x2x4 slice. The times are simulated.
32 devices in a mesh: sp: 8 (over z, y), tp: 4 (over x, core).
Axes of the slice: x: 2, y: 2, z: 4, core: 2. Of those that a mesh axis runs over, the one named last changes fastest.
Arguments:
- queries: bfloat16 [8192, 1024], P('sp', 'tp'), may hold values from -300 to 300
- keys: bfloat16 [8192, 512], P('sp', 'tp'), may hold values from -6 to 6
- values: bfloat16 [8192, 512], P('sp', 'tp'), may hold values from -6 to 6
- sink_logits: float32 [16], P('tp'), may hold values from 1 to 6
- residual: bfloat16 [8192, 2048], P('sp'), may hold values from -3 to 3
- out_weight: bfloat16 [1024, 2048], P('tp'), may hold values from -0.5390625 to 0.5390625
- norm_gain: float32 [2048], replicated, may hold values from 0.1 to 1.9
- gate_weight: bfloat16 [2048, 5632], P('sp', 'tp'), may hold values from -0.125 to 0.125
- up_weight: bfloat16 [2048, 5632], P('sp', 'tp'), may hold values from -0.125 to 0.125
- down_weight: bfloat16 [2048, 5632], P('sp', 'tp'), may hold values from -0.1796875 to 0.1796875
Outputs:
- layer_out: bfloat16 [8192, 2048], P(('sp', 'tp'))
All inputs are finite; a program needn't handle non-finite values.
Results may differ from a plain program's by a relative error of at most 0.02.
Values may be sent and summed in bfloat16 or wider, within the bound.
No kernel may reach another device: no remote copies, remote signals or barrier semaphores. Data moves between devices by JAX's collectives and lax.ppermute only.
A program may use at most 64 MiB of HBM per device.

v0:
```python
import jax
import jax.numpy as jnp
from jax import lax
from jax.sharding import PartitionSpec as P

QH = 16
HD = 64
WINDOW = 128


def shifted(block, axis, distance):
    devices = range(lax.axis_size(axis))
    route = [(i - distance, i) for i in devices if i - distance in devices]
    return lax.ppermute(block, axis, route)


def attend(queries, keys, values, sink_logits):
    local_rows = queries.shape[0]
    kv_local = keys.shape[1] // HD
    heads_local = queries.shape[1] // HD
    groups = heads_local // kv_local
    blocks = local_rows // WINDOW
    key_value = jnp.concatenate([keys, values], axis=1)
    previous = shifted(key_value[local_rows - WINDOW :], "sp", 1)
    extended = jnp.concatenate([previous, key_value], axis=0)
    stacked = extended.reshape(blocks + 1, WINDOW, 2 * kv_local * HD)
    band = jnp.concatenate([stacked[:-1], stacked[1:]], axis=1)
    key_band = band[:, :, : kv_local * HD].reshape(blocks, 2 * WINDOW, kv_local, HD)
    value_band = band[:, :, kv_local * HD :].reshape(blocks, 2 * WINDOW, kv_local, HD)
    query_blocks = queries.reshape(blocks, WINDOW, kv_local, groups, HD)
    query_index = jnp.arange(WINDOW, dtype=jnp.int32)[:, None]
    key_index = jnp.arange(2 * WINDOW, dtype=jnp.int32)[None, :]
    distance = query_index - key_index + WINDOW
    offset = lax.axis_index("sp") * local_rows
    key_place = (
        offset
        + jnp.arange(blocks, dtype=jnp.int32)[:, None, None] * WINDOW
        + key_index[None]
        - WINDOW
    )
    valid = (distance >= 0) & (distance < WINDOW) & (key_place >= 0)
    head_number = (
        lax.axis_index("tp") * heads_local + jnp.arange(heads_local, dtype=jnp.int32) + 1
    ).astype(jnp.float32)
    slopes = (2.0 ** (-8.0 * head_number / QH)).reshape(kv_local, groups, 1, 1, 1)
    scores = jnp.einsum(
        "nqhgd,nkhd->hgnqk", query_blocks, key_band, preferred_element_type=jnp.float32
    ) * HD ** (-0.5)
    scores = scores - slopes * distance.astype(jnp.float32)
    scores = jnp.where(valid, scores, -jnp.inf)
    sinks = sink_logits.reshape(kv_local, groups, 1, 1, 1)
    top = jnp.maximum(jnp.max(scores, axis=-1, keepdims=True), sinks)
    expd = jnp.exp(scores - top)
    denom = jnp.sum(expd, axis=-1, keepdims=True) + jnp.exp(sinks - top)
    weights = (expd / denom).astype(jnp.bfloat16)
    output = jnp.einsum(
        "hgnqk,nkhd->nqhgd", weights, value_band, preferred_element_type=jnp.float32
    )
    return output.reshape(local_rows, heads_local * HD).astype(jnp.bfloat16)


def rms_scale(rows, norm_gain):
    rows_f = rows.astype(jnp.float32)
    scale = lax.rsqrt(jnp.mean(rows_f * rows_f, axis=-1, keepdims=True) + 1e-06)
    return (rows_f * scale * norm_gain).astype(jnp.bfloat16)


def expand_rows(normed, gate_full, up_full):
    gate = jnp.dot(normed, gate_full, preferred_element_type=jnp.float32)
    upper = jnp.dot(normed, up_full, preferred_element_type=jnp.float32)
    return (jax.nn.silu(gate) * upper).astype(jnp.bfloat16)


def per_device(
    queries,
    keys,
    values,
    sink_logits,
    residual,
    out_weight,
    norm_gain,
    gate_weight,
    up_weight,
    down_weight,
):
    attended = attend(queries, keys, values, sink_logits)
    local_rows = queries.shape[0]
    tp_count = lax.axis_size("tp")
    own_rows = local_rows // tp_count
    first_row = lax.axis_index("tp") * own_rows
    partial_sum = jnp.dot(attended, out_weight, preferred_element_type=jnp.float32)
    projected = lax.psum(partial_sum.astype(jnp.bfloat16), "tp").astype(jnp.float32)
    mixed_all = (residual.astype(jnp.float32) + projected).astype(jnp.bfloat16)
    mixed_rows = lax.dynamic_slice_in_dim(mixed_all, first_row, own_rows, 0)
    gate_full, up_full = (
        lax.all_gather(gate_weight, "sp", axis=0, tiled=True),
        lax.all_gather(up_weight, "sp", axis=0, tiled=True),
    )
    hidden = expand_rows(rms_scale(mixed_all, norm_gain), gate_full, up_full)
    down_full = lax.all_gather(down_weight, "sp", axis=0, tiled=True)
    expanded = lax.psum_scatter(
        lax.dot_general(
            hidden, down_full, (((1,), (1,)), ((), ())), preferred_element_type=jnp.float32
        ).astype(jnp.bfloat16),
        "tp",
        scatter_dimension=0,
        tiled=True,
    ).astype(jnp.float32)
    return (mixed_rows.astype(jnp.float32) + 0.5 * expanded).astype(jnp.bfloat16)


def solution(mesh):
    return jax.shard_map(
        per_device,
        mesh=mesh,
        in_specs=(
            P("sp", "tp"),
            P("sp", "tp"),
            P("sp", "tp"),
            P("tp"),
            P("sp", None),
            P("tp", None),
            P(),
            P("sp", "tp"),
            P("sp", "tp"),
            P("sp", "tp"),
        ),
        out_specs=P(("sp", "tp"), None),
        check_vma=False,
    )
```

profile of v0, /device:TPU:0, one launch (start us, length us, event | category | flops | bytes accessed | tf_op | source)
XLA Modules:
  0.0 386.4 jit_solution(11114447815396450490)
XLA Ops:
  7.4 0.0 copy-start
  7.4 0.0 all-reduce.2.cloned.1.call-start
  7.4 1.1 constant_dynamic-update-slice_fusion.1
  8.5 1.0 constant_dynamic-update-slice_fusion
  9.5 4.9 %collective-permute-start = (bf16[128,256]{1,0:T(8,128)(2,1)S(1)}, bf16[128,256]{1,0:T(8,128)(2,1)S(1)}, u32[]{:S(2)}, u32[]{:S(2)}) collective-permute-start(bf16[128,256]{1,0:T(8,128)(2,1)S(1)} %slice.25), channel_id=1, source_target_pairs={{0,4},{4,8},{8,12},{12,16},{16,20},{20,24},{24,28},{1,5},{5,9},{9,... | collective-permute-start | bytes 196616 | tf_op jit(solution)/shard_map/ppermute | solution.py:14
  14.5 0.1 add_compare_fusion
  14.6 0.1 broadcast_multiply_fusion
  14.7 0.3 broadcast_and_fusion
  15.0 3.2 reshape.128
  18.3 0.7 max.18
  19.0 0.0 collective-permute-done
  19.1 0.3 pad_maximum_fusion
  19.3 0.2 copy.21
  19.5 2.3 fusion.5
  21.9 0.0 copy-start.1
  21.9 0.1 broadcast_maximum_fusion
  22.0 1.9 copy-done.1
  23.8 1.1 fusion.4
  24.9 0.1 exponential_add_fusion
  25.0 0.2 copy.20
  25.3 3.5 fusion.11
  28.7 0.3 copy.26
  29.1 0.0 copy-done
  29.1 3.3 convolution_convert_fusion.1
  32.4 0.0 all-reduce.2.cloned.1.call-update
  32.4 0.0 all-gather.4.cloned.1.call-start
  32.5 0.5 all-gather.4.cloned.1.call-update
  33.0 0.0 all-gather.6.cloned.1.call-start
  33.0 0.5 all-gather.6.cloned.1.call-update
  33.6 0.0 all-gather.8.cloned.1.call-start
  33.6 0.5 all-gather.8.cloned.1.call-update
  34.2 0.0 copy-start.2
  34.2 0.2 reduce-scatter.2.cloned.1.call-start
  34.4 83.9 %all-reduce.2.cloned.1.call-done = bf16[1024,2048]{1,0:T(8,128)(2,1)} async-done(((bf16[1024,2048]{1,0:T(8,128)(2,1)}), bf16[1024,2048]{1,0:T(8,128)(2,1)}) %all-reduce.2.cloned.1.call-update) | async-done | bytes 4194320 | tf_op jit(solution)/shard_map/psum | solution.py:92
  118.4 7.5 %fusion = (f32[1024]{0:T(1024)S(1)}, bf16[1024,2048]{1,0:T(8,128)(2,1)}) fusion(bf16[1024,2048]{1,0:T(8,128)(2,1)} %all-reduce.2.cloned.1.call-done, bf16[1024,2048]{1,0:T(8,128)(2,1)} %param.14), kind=kLoop, calls=%fused_computation.2 | loop fusion | flops 14679040 | bytes 12587008 | tf_op jit(solution)/shard_map/reduce_sum | solution.py:64
  125.8 1.7 all-gather.4.cloned.1.call-done
  127.5 0.0 copy-done.2
  127.5 11.9 %fusion.15 = f32[1024,1408]{1,0:T(8,128)} fusion(bf16[2048,1408]{1,0:T(8,128)(2,1)} %all-gather.4.cloned.1.call-done, bf16[1024,2048]{1,0:T(8,128)(2,1)} %get-tuple-element.6, f32[2048]{0:T(1024)S(1)} %copy-done.2, f32[1024]{0:T(1024)S(1)} %add_rsqrt_fusion), kind=kOutput, calls=%fused_computation.20 | convolution fusion | flops 5913968640 | bytes 15740928 | tf_op jit(solution)/shard_map/dot_general | solution.py:69
  139.5 80.4 %all-gather.6.cloned.1.call-done = bf16[2048,1408]{1,0:T(8,128)(2,1)} async-done(((bf16[256,1408]{1,0:T(8,128)(2,1)}), bf16[2048,1408]{1,0:T(8,128)(2,1)}) %all-gather.6.cloned.1.call-update) | async-done | bytes 5767184 | tf_op jit(solution)/shard_map/all_gather | solution.py:97
  219.9 92.4 %all-gather.8.cloned.1.call-done = bf16[2048,1408]{1,0:T(8,128)(2,1)} async-done(((bf16[256,1408]{1,0:T(8,128)(2,1)}), bf16[2048,1408]{1,0:T(8,128)(2,1)}) %all-gather.8.cloned.1.call-update) | async-done | bytes 5767184 | tf_op jit(solution)/shard_map/all_gather | solution.py:100
  312.2 20.8 %convolution_convert_fusion = bf16[1024,2048]{1,0:T(8,128)(2,1)} fusion(bf16[2048,1408]{1,0:T(8,128)(2,1)} %all-gather.8.cloned.1.call-done, f32[1024,1408]{1,0:T(8,128)} %fusion.15, bf16[2048,1408]{1,0:T(8,128)(2,1)} %all-gather.6.cloned.1.call-done, bf16[1024,2048]{1,0:T(8,128)(2,1)} %get-tuple-element.6, f32[2048]{0:T(1024)S(1)} %copy-done.2, ...), kind=kOutput, calls=%fused_computation.11 | convolution fusion | flops 11830296576 | bytes 25702400 | tf_op jit(solution)/shard_map/dot_general | solution.py:102
  333.1 0.0 reduce-scatter.2.cloned.1.call-update
  333.1 42.8 %reduce-scatter.2.cloned.1.call-done = bf16[256,2048]{1,0:T(8,128)(2,1)} async-done(((bf16[1024,2048]{1,0:T(8,128)(2,1)}), bf16[256,2048]{1,0:T(8,128)(2,1)}) %reduce-scatter.2.cloned.1.call-update) | async-done | bytes 1048592 | tf_op jit(solution)/shard_map/reduce_scatter | solution.py:101
  375.9 2.9 add_convert_fusion.1
  (7 shorter events, 0.1 us)
Async XLA Ops:
  7.4 21.7 %copy-start = (bf16[256,2048]{1,0:T(8,128)(2,1)S(1)}, bf16[256,2048]{1,0:T(8,128)(2,1)}, u32[]{:S(2)}) copy-start(bf16[256,2048]{1,0:T(8,128)(2,1)} %param.15) | copy-start | bytes 3145732
  7.4 111.0 %all-reduce.2.cloned.1.call-start = ((), (), s32[]{:S(2)}) async-start(), calls=%async_computation.1 | async-start | bytes 8388608 | tf_op jit(solution)/shard_map/psum | solution.py:92
  9.5 9.5 %collective-permute-start = (bf16[128,256]{1,0:T(8,128)(2,1)S(1)}, bf16[128,256]{1,0:T(8,128)(2,1)S(1)}, u32[]{:S(2)}, u32[]{:S(2)}) collective-permute-start(bf16[128,256]{1,0:T(8,128)(2,1)S(1)} %slice.25), channel_id=1, source_target_pairs={{0,4},{4,8},{8,12},{12,16},{16,20},{20,24},{24,28},{1,5},{5,9},{9,... | collective-permute-start | bytes 196616 | tf_op jit(solution)/shard_map/ppermute | solution.py:14
  21.9 1.9 copy-start.1
  32.4 95.1 %all-gather.4.cloned.1.call-start = ((), (), s32[]{:S(2)}) async-start(), calls=%async_computation.2 | async-start | bytes 6488064 | tf_op jit(solution)/shard_map/all_gather | solution.py:96
  33.0 186.9 %all-gather.6.cloned.1.call-start = ((), (), s32[]{:S(2)}) async-start(), calls=%async_computation.3 | async-start | bytes 6488064 | tf_op jit(solution)/shard_map/all_gather | solution.py:97
  33.6 278.7 %all-gather.8.cloned.1.call-start = ((), (), s32[]{:S(2)}) async-start(), calls=%async_computation.4 | async-start | bytes 6488064 | tf_op jit(solution)/shard_map/all_gather | solution.py:100
  34.2 93.4 %copy-start.2 = (f32[2048]{0:T(1024)S(1)}, f32[2048]{0:T(1024)}, u32[]{:S(2)}) copy-start(f32[2048]{0:T(1024)} %param.16) | copy-start | bytes 24580
  34.2 341.8 %reduce-scatter.2.cloned.1.call-start = ((), (), s32[]{:S(2)}) async-start(), calls=%async_computation.5 | async-start | bytes 5242880 | tf_op jit(solution)/shard_map/reduce_scatter | solution.py:101
Sparse Core Ops, SparseCore 0:
  32.5 85.7 all-reduce.1
  333.2 42.6 reduce-scatter.1
Sparse Core Ops, SparseCore 1:
  35.1 92.4 all-gather.3
  129.6 90.2 all-gather.5
  222.0 90.2 all-gather.7
where the time goes:
time: 387 us; the launch traced here: 386 us
  waiting for transfers between devices  303 us (78%)
  matrix products  41.9 us (11%)
  between operations  15.2 us (4%)
  other arithmetic  12.5 us (3%)
  local copies, waits for them, and re-layouts  8.71 us (2%)
  starting transfers between devices  5.25 us (1%)
    all_gather x1, waiting for transfers between devices, per_device(): down_full = lax.all_gather(down_weight, 'sp', axis=0, tiled=True)  92.4 us
    psum x1, waiting for transfers between devices, per_device(): lax.psum(partial_sum.astype(jnp.bfloat16), 'tp').astype(jnp.float32)  83.9 us
    all_gather x1, waiting for transfers between devices, per_device(): lax.all_gather(up_weight, 'sp', axis=0, tiled=True)  80.4 us
    reduce_scatter x1, waiting for transfers between devices, per_device(): lax.psum_scatter(lax.dot_general(hidden, down_full, (((1,), (1,)), ((), (...  42.8 us
    dot_general x1, matrix products, per_device(): lax.dot_general(hidden, down_full, (((1,), (1,)), ((), ())), preferred_el...  20.8 us
    dot_general x1, matrix products, expand_rows(): gate = jnp.dot(normed, gate_full, preferred_element_type=jnp.float32)  11.9 us
  transfers between devices with their start and end apart: 6, of which 5 were waited for; matrix products, arithmetic and copies ran while one was open for 6% of the time, Pallas kernels for 0%

commit v1 on v0

--- a/solution.py
+++ b/solution.py
@@ -1,6 +1,8 @@
 import jax
 import jax.numpy as jnp
 from jax import lax
+from jax.experimental import pallas as pl
+from jax.experimental.pallas import tpu as pltpu
 from jax.sharding import PartitionSpec as P
 
 QH = 16
@@ -65,10 +67,108 @@
     return (rows_f * scale * norm_gain).astype(jnp.bfloat16)
 
 
-def expand_rows(normed, gate_full, up_full):
-    gate = jnp.dot(normed, gate_full, preferred_element_type=jnp.float32)
-    upper = jnp.dot(normed, up_full, preferred_element_type=jnp.float32)
-    return (jax.nn.silu(gate) * upper).astype(jnp.bfloat16)
+def pair_route(axis):
+    return [(i, i ^ 1) for i in range(lax.axis_size(axis))]
+
+
+def across_route(axis, step):
+    count = lax.axis_size(axis)
+    return [(i, (i + 2 * step) % count) for i in range(count)]
+
+
+def hop(block, axis, step):
+    route = across_route(axis, step) if step else pair_route(axis)
+    return lax.ppermute(block, axis, route)
+
+
+def gather_ring(block, lines):
+    half = block.shape[0] // 2
+    reach = lines // 2
+    ahead, behind = [block], [block]
+    for _ in range(1, reach):
+        ahead.append(hop(ahead[-1], "sp", -1))
+        behind.append(hop(behind[-1], "sp", 1))
+    front = hop(ahead[-1][:half], "sp", -1)
+    back = hop(behind[-1][half:], "sp", 1)
+    own = hop(block, "sp", 0)
+    ahead_side = [own] + [hop(ahead[k], "sp", 0) for k in range(1, reach)]
+    behind_side = [hop(behind[k], "sp", 0) for k in range(1, reach)]
+    front_side = hop(front, "sp", 0)
+    back_side = hop(ahead_side[-1][half:], "sp", -1)
+    same = ahead + [front, back] + behind[:0:-1]
+    other = ahead_side + [front_side, back_side] + behind_side[::-1]
+    return same, other
+
+
+def add_up(kept, given, chips, own_rows):
+    total = kept.astype(jnp.float32) + hop(given, "tp", 0).astype(jnp.float32)
+    pieces = []
+    for step in range(1, chips):
+        piece = total[step * own_rows : (step + 1) * own_rows].astype(jnp.bfloat16)
+        pieces.append(hop(piece, "tp", step))
+    return [total[:own_rows]] + pieces
+
+
+def added(terms):
+    total = terms[0]
+    for term in terms[1:]:
+        total = total + term.astype(jnp.float32)
+    return total
+
+
+def close(mixed, same, other, side, spot, lines, shard):
+    rows, width = mixed.shape
+    if shard % 128:
+        sums = [
+            turned(added(terms).reshape(rows, lines, 1, shard), (lines - spot) % lines, 1)
+            for terms in (same, other)
+        ]
+        first = jnp.where(side == 0, sums[0], sums[1])
+        second = jnp.where(side == 0, sums[1], sums[0])
+        expanded = jnp.concatenate([first, second], axis=2).reshape(rows, width)
+        return (mixed.astype(jnp.float32) + 0.5 * expanded).astype(jnp.bfloat16)
+    count = len(same)
+
+    def body(where, mixed_ref, *refs):
+        out_ref = refs[-1]
+        near = added([ref[...] for ref in refs[:count]])
+        far = added([ref[...] for ref in refs[count:-1]])
+        mine = pl.program_id(0) % 2 == where[0]
+        expanded = jnp.where(mine, near, far)
+        out_ref[...] = (mixed_ref[...].astype(jnp.float32) + 0.5 * expanded).astype(jnp.bfloat16)
+
+    def source(j, where):
+        return 0, (j // 2 + lines - where[1]) % lines
+
+    def place(j, where):
+        return 0, j
+
+    spec = pl.BlockSpec((rows, shard), source)
+    return pl.pallas_call(
+        body,
+        grid_spec=pltpu.PrefetchScalarGridSpec(
+            num_scalar_prefetch=1,
+            grid=(2 * lines,),
+            in_specs=[pl.BlockSpec((rows, shard), place)] + [spec] * (2 * count),
+            out_specs=pl.BlockSpec((rows, shard), place),
+        ),
+        out_shape=jax.ShapeDtypeStruct((rows, width), jnp.bfloat16),
+    )(jnp.stack([side, spot]).astype(jnp.int32), mixed, *same, *other)
+
+
+def dot_rows(rows, matrix):
+    return jnp.dot(rows, matrix, preferred_element_type=jnp.float32)
+
+
+def dot_back(rows, matrix):
+    return lax.dot_general(
+        rows, matrix, (((1,), (1,)), ((), ())), preferred_element_type=jnp.float32
+    ).astype(jnp.bfloat16)
+
+
+def turned(block, start, axis):
+    size = block.shape[axis]
+    return lax.dynamic_slice_in_dim(jnp.concatenate([block, block], axis), start, size, axis)
 
 
 def per_device(
@@ -83,30 +183,63 @@
     up_weight,
     down_weight,
 ):
-    attended = attend(queries, keys, values, sink_logits)
     local_rows = queries.shape[0]
     tp_count = lax.axis_size("tp")
+    chips = tp_count // 2
     own_rows = local_rows // tp_count
-    first_row = lax.axis_index("tp") * own_rows
-    partial_sum = jnp.dot(attended, out_weight, preferred_element_type=jnp.float32)
-    projected = lax.psum(partial_sum.astype(jnp.bfloat16), "tp").astype(jnp.float32)
-    mixed_all = (residual.astype(jnp.float32) + projected).astype(jnp.bfloat16)
-    mixed_rows = lax.dynamic_slice_in_dim(mixed_all, first_row, own_rows, 0)
-    gate_full, up_full = (
-        lax.all_gather(gate_weight, "sp", axis=0, tiled=True),
-        lax.all_gather(up_weight, "sp", axis=0, tiled=True),
-    )
-    hidden = expand_rows(rms_scale(mixed_all, norm_gain), gate_full, up_full)
-    down_full = lax.all_gather(down_weight, "sp", axis=0, tiled=True)
-    expanded = lax.psum_scatter(
-        lax.dot_general(
-            hidden, down_full, (((1,), (1,)), ((), ())), preferred_element_type=jnp.float32
-        ).astype(jnp.bfloat16),
-        "tp",
-        scatter_dimension=0,
-        tiled=True,
-    ).astype(jnp.float32)
-    return (mixed_rows.astype(jnp.float32) + 0.5 * expanded).astype(jnp.bfloat16)
+    place = lax.axis_index("tp")
+    core = place % 2
+    side = lax.axis_index("sp") % 2
+    spot = lax.axis_index("sp") // 2
+    shard = gate_weight.shape[0]
+    lines = lax.axis_size("sp") // 2
+    half = lines * shard
+    gate_same, gate_other = gather_ring(gate_weight, lines)
+    up_same, up_other = gather_ring(up_weight, lines)
+    down_same, down_other = gather_ring(down_weight, lines)
+
+    attended = attend(queries, keys, values, sink_logits)
+    by_place = turned(attended.reshape(chips, 2, own_rows, attended.shape[1]), place // 2, 0)
+    kept_rows = lax.dynamic_index_in_dim(by_place, core, 1, False)
+    given_rows = lax.dynamic_index_in_dim(by_place, 1 - core, 1, False)
+    flat = (chips * own_rows, attended.shape[1])
+    given = dot_rows(given_rows.reshape(flat), out_weight).astype(jnp.bfloat16)
+    kept = dot_rows(kept_rows.reshape(flat), out_weight).astype(jnp.bfloat16)
+    projected = added(add_up(kept, given, chips, own_rows))
+    residual_rows = lax.dynamic_slice_in_dim(residual, place * own_rows, own_rows, 0)
+    mixed = (residual_rows.astype(jnp.float32) + projected).astype(jnp.bfloat16)
+
+    normed = turned(rms_scale(mixed, norm_gain).reshape(own_rows, lines, 2, shard), spot, 1)
+    normed = jnp.concatenate(
+        [
+            lax.dynamic_index_in_dim(normed, side, 2, False).reshape(own_rows, half),
+            lax.dynamic_index_in_dim(normed, 1 - side, 2, False).reshape(own_rows, half),
+        ],
+        axis=1,
+    )
+    pieces = [normed] + [hop(normed, "tp", -k) for k in range(1, chips)]
+    near = jnp.concatenate(pieces, axis=0)
+    rows = jnp.concatenate([near, hop(near, "tp", 0)], axis=0)
+    gates, uppers = [], []
+    for name, blocks, into in (
+        ("gate_one", gate_same, gates),
+        ("up_one", up_same, uppers),
+        ("gate_two", gate_other, gates),
+    ):
+        source = rows[:, half:] if name == "gate_two" else rows[:, :half]
+        into.append(dot_rows(source, jnp.concatenate(blocks, axis=0)))
+    uppers.append(dot_rows(rows[:, half:], jnp.concatenate(up_other, axis=0)))
+    gate = gates[0] + gates[1]
+    upper = uppers[0] + uppers[1]
+    hidden = (jax.nn.silu(gate) * upper).astype(jnp.bfloat16)
+    split = chips * own_rows
+    sums = []
+    for blocks in (down_same, down_other):
+        matrix = jnp.concatenate(blocks, axis=0)
+        given = dot_back(hidden[split:], matrix)
+        kept = dot_back(hidden[:split], matrix)
+        sums.append(add_up(kept, given, chips, own_rows))
+    return close(mixed, sums[0], sums[1], side, spot, lines, shard)
 
 
 def solution(mesh):

time: 387 us -> 340 us (0.88)
  waiting for transfers between devices: 303 us -> 140 us
  starting transfers between devices: 5.25 us -> 89.5 us
  local copies, waits for them, and re-layouts: 8.71 us -> 53 us
  between operations: 15.2 us -> 0.8 us
  Pallas kernels: 0 us -> 6.92 us
  matrix products: 41.9 us -> 37.9 us
    all_gather x3 -> x0, waiting for transfers between devices: 174 us -> none  [the longest x1 92.4 us: per_device(): down_full = lax.all_gather(down_weight, 'sp', axis=0, tiled=True)]
    ppermute x0 -> x35, waiting for transfers between devices: none -> 133 us  [hop(): return lax.ppermute(block, axis, route)]
    ppermute x0 -> x35, starting transfers between devices: none -> 87.1 us  [hop(): return lax.ppermute(block, axis, route)]
    psum x1 -> x0, waiting for transfers between devices: 83.9 us -> none  [per_device(): lax.psum(partial_sum.astype(jnp.bfloat16), 'tp').astype(jnp.float32)]
    reduce_scatter x1 -> x0, waiting for transfers between devices: 42.8 us -> none  [per_device(): lax.psum_scatter(lax.dot_general(hidden, down_full, (((1,), (1,)), ((), (...]
    unnamed x7 -> x88, local copies, waits for them, and re-layouts: 2.95 us -> 28.8 us
    slice x0 -> x14, local copies, waits for them, and re-layouts: none -> 10.3 us  [the longest x3 3.04 us: gather_ring(): back_side = hop(ahead_side[-1][half:], 'sp', -1)]
    ppermute x1, waiting for transfers between devices: 0.01 us -> 7.59 us  [shifted(): return lax.ppermute(block, axis, route)]
  transfers between devices with their start and end apart: 6 -> 36, of which waited for: 5 -> 18; matrix products, arithmetic and copies ran while one was open for 6% -> 21% of each run, Pallas kernels for 0% -> 0%
where the time goes in v1:
time: 340 us; the launch traced here: 339 us
  waiting for transfers between devices  140 us (41%)
  starting transfers between devices  89.5 us (26%)
  local copies, waits for them, and re-layouts  53 us (16%)
  matrix products  37.9 us (11%)
  other arithmetic  10.9 us (3%)
  Pallas kernels  6.92 us (2%)
    ppermute x35, waiting for transfers between devices, hop(): return lax.ppermute(block, axis, route)  133 us
    ppermute x35, starting transfers between devices, hop(): return lax.ppermute(block, axis, route)  87.1 us
    unnamed x88, local copies, waits for them, and re-layouts  28.8 us
    dot_general x6, matrix products, dot_rows(): return jnp.dot(rows, matrix, preferred_element_type=jnp.float32)  23.3 us
    dot_general x4, matrix products, dot_back(): lax.dot_general(rows, matrix, (((1,), (1,)), ((), ())), preferred_element...  8.8 us
    ppermute x1, waiting for transfers between devices, shifted(): return lax.ppermute(block, axis, route)  7.59 us
    pallas_call x1, Pallas kernels, close(): pl.pallas_call(body, grid_spec=pltpu.PrefetchScalarGridSpec(num_scalar_pr...  6.92 us
  transfers between devices with their start and end apart: 36, of which 18 were waited for; matrix products, arithmetic and copies ran while one was open for 21% of the time, Pallas kernels for 0%

profile of v1, /device:TPU:0, one launch (start us, length us, event | category | flops | bytes accessed | tf_op | source)
XLA Modules:
  0.0 339.2 jit_solution(6355401229783365274)
XLA Ops:
  0.0 5.1 %collective-permute-start.5 = (bf16[256,1408]{1,0:T(8,128)(2,1)}, bf16[256,1408]{1,0:T(8,128)(2,1)}, u32[]{:S(2)}, u32[]{:S(2)}) collective-permute-start(bf16[256,1408]{1,0:T(8,128)(2,1)} %param.17), channel_id=1, source_target_pairs={{0,24},{4,28},{8,0},{12,4},{16,8},{20,12},{24,16},{28,20},{1,25},{... | collective-permute-start | bytes 2162696 | tf_op jit(solution)/shard_map/ppermute | solution.py:81
  8.7 2.4 collective-permute-start
  12.2 2.0 constant_dynamic-update-slice_fusion.8
  17.2 7.6 %collective-permute-done = bf16[128,256]{1,0:T(8,128)(2,1)S(1)} collective-permute-done((bf16[128,256]{1,0:T(8,128)(2,1)S(1)}, bf16[128,256]{1,0:T(8,128)(2,1)S(1)}, u32[]{:S(2)}, u32[]{:S(2)}) %collective-permute-start) | collective-permute-done | bytes 65568 | tf_op jit(solution)/shard_map/ppermute | solution.py:16
  25.3 2.3 fusion.2
  27.8 2.0 copy-done.3
  31.2 3.5 %fusion.24 = bf16[8,128,2,2,64]{1,4,3,2,0:T(8,128)(2,1)S(1)} fusion(bf16[8,256,2,64,1]{1,3,4,2,0:T(8,128)(2,1)S(1)} %bitcast.57, f32[2,8,256,128,2]{3,2,4,1,0:T(8,128)} %copy-done.3, f32[2,2,8,128]{3,1,2,0:T(2,128)S(1)} %exponential_add_fusion, f32[2,2,8,128]{3,1,2,0:T(2,128)S(1)} %broadcast_maximum_fusion, ...), kind=kOutput, calls=%fused_computation.45 | convolution fusion | flops 140771328 | bytes 6062080 | tf_op jit(solution)/shard_map/hgnqk,nkhd->nqhgd/dot_general | solution.py:58
  38.5 2.1 convolution_convert_fusion
  40.6 2.1 constant_dynamic-update-slice_fusion.28
  43.9 16.7 %collective-permute-start.14 = (bf16[256,1408]{1,0:T(8,128)(2,1)}, bf16[256,1408]{1,0:T(8,128)(2,1)}, u32[]{:S(2)}, u32[]{:S(2)}) collective-permute-start(bf16[256,1408]{1,0:T(8,128)(2,1)} %param.18), channel_id=1, source_target_pairs={{0,24},{4,28},{8,0},{12,4},{16,8},{20,12},{24,16},{28,20},{1,25},{... | collective-permute-start | bytes 2162696 | tf_op jit(solution)/shard_map/ppermute | solution.py:81
  61.7 2.2 constant_dynamic-update-slice_fusion.13
  63.9 2.0 constant_dynamic-update-slice_fusion.7
  66.4 2.0 constant_dynamic-update-slice_fusion.23
  70.0 10.2 %collective-permute-done.29 = bf16[256,1408]{1,0:T(8,128)(2,1)S(1)} collective-permute-done((bf16[256,1408]{1,0:T(8,128)(2,1)}, bf16[256,1408]{1,0:T(8,128)(2,1)S(1)}, u32[]{:S(2)}, u32[]{:S(2)}) %collective-permute-start.29) | collective-permute-done | bytes 720928 | tf_op jit(solution)/shard_map/ppermute | solution.py:81
  81.2 3.8 %collective-permute-start.6 = (bf16[128,1408]{1,0:T(8,128)(2,1)S(1)}, bf16[128,1408]{1,0:T(8,128)(2,1)S(1)}, u32[]{:S(2)}, u32[]{:S(2)}) collective-permute-start(bf16[128,1408]{1,0:T(8,128)(2,1)S(1)} %slice.114), channel_id=1, source_target_pairs={{0,24},{4,28},{8,0},{12,4},{16,8},{20,12},{24,16},{28,20},{1,25},{... | collective-permute-start | bytes 1081352 | tf_op jit(solution)/shard_map/ppermute | solution.py:81
  87.2 5.9 %collective-permute-done.23 = bf16[256,1408]{1,0:T(8,128)(2,1)} collective-permute-done((bf16[256,1408]{1,0:T(8,128)(2,1)S(1)}, bf16[256,1408]{1,0:T(8,128)(2,1)}, u32[]{:S(2)}, u32[]{:S(2)}) %collective-permute-start.23) | collective-permute-done | bytes 720928 | tf_op jit(solution)/shard_map/ppermute | solution.py:81
  93.1 32.8 %collective-permute-start.8 = (bf16[128,1408]{1,0:T(8,128)(2,1)S(1)}, bf16[128,1408]{1,0:T(8,128)(2,1)S(1)}, u32[]{:S(2)}, u32[]{:S(2)}) collective-permute-start(bf16[128,1408]{1,0:T(8,128)(2,1)S(1)} %slice.115), channel_id=1, source_target_pairs={{0,8},{4,12},{8,16},{12,20},{16,24},{20,28},{24,0},{28,4},{1,9},{5... | collective-permute-start | bytes 1081352 | tf_op jit(solution)/shard_map/ppermute | solution.py:81
  125.9 2.0 constant_dynamic-update-slice_fusion.27
  130.1 2.1 collective-permute-start.17
  132.9 2.8 collective-permute-start.24
  136.6 3.6 %collective-permute-done.8 = bf16[128,1408]{1,0:T(8,128)(2,1)S(1)} collective-permute-done((bf16[128,1408]{1,0:T(8,128)(2,1)S(1)}, bf16[128,1408]{1,0:T(8,128)(2,1)S(1)}, u32[]{:S(2)}, u32[]{:S(2)}) %collective-permute-start.8) | collective-permute-done | bytes 360480 | tf_op jit(solution)/shard_map/ppermute | solution.py:81
  143.8 4.1 %collective-permute-done.15 = bf16[128,1408]{1,0:T(8,128)(2,1)S(1)} collective-permute-done((bf16[128,1408]{1,0:T(8,128)(2,1)S(1)}, bf16[128,1408]{1,0:T(8,128)(2,1)S(1)}, u32[]{:S(2)}, u32[]{:S(2)}) %collective-permute-start.15) | collective-permute-done | bytes 360480 | tf_op jit(solution)/shard_map/ppermute | solution.py:81
  149.5 6.2 %collective-permute-done.17 = bf16[128,1408]{1,0:T(8,128)(2,1)S(1)} collective-permute-done((bf16[128,1408]{1,0:T(8,128)(2,1)S(1)}, bf16[128,1408]{1,0:T(8,128)(2,1)S(1)}, u32[]{:S(2)}, u32[]{:S(2)}) %collective-permute-start.17) | collective-permute-done | bytes 360480 | tf_op jit(solution)/shard_map/ppermute | solution.py:81
  155.7 6.8 %collective-permute-done.24 = bf16[128,1408]{1,0:T(8,128)(2,1)S(1)} collective-permute-done((bf16[128,1408]{1,0:T(8,128)(2,1)S(1)}, bf16[128,1408]{1,0:T(8,128)(2,1)S(1)}, u32[]{:S(2)}, u32[]{:S(2)}) %collective-permute-start.24) | collective-permute-done | bytes 360480 | tf_op jit(solution)/shard_map/ppermute | solution.py:81
  163.3 2.0 constant_dynamic-update-slice_fusion.4
  165.5 5.9 %collective-permute-done.2 = bf16[256,2048]{1,0:T(8,128)(2,1)S(1)} collective-permute-done((bf16[256,2048]{1,0:T(8,128)(2,1)S(1)}, bf16[256,2048]{1,0:T(8,128)(2,1)S(1)}, u32[]{:S(2)}, u32[]{:S(2)}) %collective-permute-start.2) | collective-permute-done | bytes 1048608 | tf_op jit(solution)/shard_map/ppermute | solution.py:81
  177.6 2.0 constant_dynamic-update-slice_fusion.25
  180.5 2.1 collective-permute-start.22
  183.7 9.0 %collective-permute-done.19 = bf16[256,1408]{1,0:T(8,128)(2,1)} collective-permute-done((bf16[256,1408]{1,0:T(8,128)(2,1)}, bf16[256,1408]{1,0:T(8,128)(2,1)}, u32[]{:S(2)}, u32[]{:S(2)}) %collective-permute-start.19) | collective-permute-done | bytes 720928 | tf_op jit(solution)/shard_map/ppermute | solution.py:81
  194.3 14.0 %collective-permute-done.30 = bf16[256,1408]{1,0:T(8,128)(2,1)} collective-permute-done((bf16[256,1408]{1,0:T(8,128)(2,1)}, bf16[256,1408]{1,0:T(8,128)(2,1)}, u32[]{:S(2)}, u32[]{:S(2)}) %collective-permute-start.30) | collective-permute-done | bytes 720928 | tf_op jit(solution)/shard_map/ppermute | solution.py:81
  208.5 2.1 constant_dynamic-update-slice_fusion.32
  214.6 16.7 %collective-permute-done.11 = bf16[128,1408]{1,0:T(8,128)(2,1)S(1)} collective-permute-done((bf16[128,1408]{1,0:T(8,128)(2,1)S(1)}, bf16[128,1408]{1,0:T(8,128)(2,1)S(1)}, u32[]{:S(2)}, u32[]{:S(2)}) %collective-permute-start.11) | collective-permute-done | bytes 360480 | tf_op jit(solution)/shard_map/ppermute | solution.py:81
  231.3 7.7 %collective-permute-done.20 = bf16[128,1408]{1,0:T(8,128)(2,1)S(1)} collective-permute-done((bf16[128,1408]{1,0:T(8,128)(2,1)S(1)}, bf16[128,1408]{1,0:T(8,128)(2,1)S(1)}, u32[]{:S(2)}, u32[]{:S(2)}) %collective-permute-start.20) | collective-permute-done | bytes 360480 | tf_op jit(solution)/shard_map/ppermute | solution.py:81
  240.3 4.4 %collective-permute-done.31 = bf16[128,1408]{1,0:T(8,128)(2,1)S(1)} collective-permute-done((bf16[128,1408]{1,0:T(8,128)(2,1)S(1)}, bf16[128,1408]{1,0:T(8,128)(2,1)S(1)}, u32[]{:S(2)}, u32[]{:S(2)}) %collective-permute-start.31) | collective-permute-done | bytes 360480 | tf_op jit(solution)/shard_map/ppermute | solution.py:81
  244.7 2.6 collective-permute-start.21
  248.3 2.7 collective-permute-start.32
  251.1 5.0 %collective-permute-done.21 = bf16[128,1408]{1,0:T(8,128)(2,1)S(1)} collective-permute-done((bf16[128,1408]{1,0:T(8,128)(2,1)S(1)}, bf16[128,1408]{1,0:T(8,128)(2,1)S(1)}, u32[]{:S(2)}, u32[]{:S(2)}) %collective-permute-start.21) | collective-permute-done | bytes 360480 | tf_op jit(solution)/shard_map/ppermute | solution.py:81
  256.4 5.8 %collective-permute-done.32 = bf16[128,1408]{1,0:T(8,128)(2,1)S(1)} collective-permute-done((bf16[128,1408]{1,0:T(8,128)(2,1)S(1)}, bf16[128,1408]{1,0:T(8,128)(2,1)S(1)}, u32[]{:S(2)}, u32[]{:S(2)}) %collective-permute-start.32) | collective-permute-done | bytes 360480 | tf_op jit(solution)/shard_map/ppermute | solution.py:81
  263.6 7.5 %collective-permute-done.33 = bf16[256,1408]{1,0:T(8,128)(2,1)S(1)} collective-permute-done((bf16[256,1408]{1,0:T(8,128)(2,1)S(1)}, bf16[256,1408]{1,0:T(8,128)(2,1)S(1)}, u32[]{:S(2)}, u32[]{:S(2)}) %collective-permute-start.33) | collective-permute-done | bytes 720928 | tf_op jit(solution)/shard_map/ppermute | solution.py:81
  271.2 4.5 %pad_maximum_fusion = bf16[1024,2048]{0,1:T(8,128)(2,1)S(1)} fusion(bf16[512,2048]{0,1:T(8,128)(2,1)S(1)} %collective-permute-done.4, bf16[256,2048]{0,1:T(8,128)(2,1)S(1)} %collective-permute-done.3, bf16[256,1024]{0,1:T(8,128)(2,1)S(1)} %bitcast.52, bf16[256,1024]{0,1:T(8,128)(2,1)S(1)} %bitcast.49), kind=kLoop, calls=%fused_computation.1 | loop fusion | flops 16777216 | bytes 8388608 | tf_op jit(solution)/shard_map/concatenate | solution.py:222
  275.7 3.5 %fusion.11 = f32[1024,1408]{1,0:T(8,128)S(1)} fusion(bf16[1024,1408]{1,0:T(8,128)(2,1)S(1)} %constant_dynamic-update-slice_fusion.9, bf16[1024,2048]{0,1:T(8,128)(2,1)S(1)} %pad_maximum_fusion), kind=kOutput, calls=%fused_computation.30 | convolution fusion | flops 2952790016 | bytes 10747904 | tf_op jit(solution)/shard_map/dot_general | solution.py:160
  279.3 3.6 %fusion.15 = f32[1024,1408]{1,0:T(8,128)S(1)} fusion(bf16[1024,1408]{1,0:T(8,128)(2,1)S(1)} %copy-done.23, bf16[1024,2048]{0,1:T(8,128)(2,1)S(1)} %pad_maximum_fusion), kind=kOutput, calls=%fused_computation.34 | convolution fusion | flops 2952790016 | bytes 10747904 | tf_op jit(solution)/shard_map/dot_general | solution.py:160
  282.9 5.3 %fusion.13 = f32[1024,1408]{1,0:T(8,128)} fusion(bf16[1024,1408]{1,0:T(8,128)(2,1)S(1)} %copy-done.22, bf16[1024,2048]{0,1:T(8,128)(2,1)S(1)} %pad_maximum_fusion), kind=kOutput, calls=%fused_computation.32 | convolution fusion | flops 2952790016 | bytes 10747904 | tf_op jit(solution)/shard_map/dot_general | solution.py:160
  288.2 8.1 %multiply_convert_fusion = bf16[1024,1408]{1,0:T(8,128)(2,1)} fusion(f32[1024,1408]{1,0:T(8,128)} %fusion.13, f32[1024,1408]{1,0:T(8,128)S(1)} %fusion.15, f32[1024,1408]{1,0:T(8,128)S(1)} %fusion.11, bf16[1024,1408]{1,0:T(8,128)(2,1)S(1)} %constant_dynamic-update-slice_fusion.19, bf16[1024,2048]{0,1:T(8,128)(2,1)S(1)} %pad_maximum_fusion), kind=kOutput, calls=%fused_computation | convolution fusion | flops 2964324352 | bytes 25165824 | tf_op jit(solution)/shard_map/dot_general | solution.py:160
  296.3 3.3 convolution_convert_fusion.2
  311.7 9.5 %collective-permute-done.35.refs_3_ = bf16[256,1024]{1,0:T(8,128)(2,1)S(1)} collective-permute-done((bf16[256,1024]{1,0:T(8,128)(2,1)S(1)}, bf16[256,1024]{1,0:T(8,128)(2,1)S(1)}, u32[]{:S(2)}, u32[]{:S(2)}) %collective-permute-start.35) | collective-permute-done | bytes 524320 | tf_op jit(solution)/shard_map/ppermute | solution.py:81
  321.1 10.3 %collective-permute-done.28.refs_1_ = bf16[256,1024]{1,0:T(8,128)(2,1)S(1)} collective-permute-done((bf16[256,1024]{1,0:T(8,128)(2,1)S(1)}, bf16[256,1024]{1,0:T(8,128)(2,1)S(1)}, u32[]{:S(2)}, u32[]{:S(2)}) %collective-permute-start.28) | collective-permute-done | bytes 524320 | tf_op jit(solution)/shard_map/ppermute | solution.py:81
  332.2 6.9 %shard_map.100 = bf16[256,2048]{1,0:T(8,128)(2,1)} custom-call(s32[2]{0:T(128)} %pad_add_fusion.where, bf16[256,2048]{1,0:T(8,128)(2,1)} %copy-done.2, f32[256,1024]{1,0:T(8,128)} %slice.125.refs_0_, bf16[256,1024]{1,0:T(8,128)(2,1)} %copy-done.13, f32[256,1024]{1,0:T(8,128)} %slice.128.refs_2_, bf16[256,1024]{1,0:T(8,128)(2,1)} %copy-done.12), custom_call_target="tpu_custom_call" | custom-call | tf_op jit(solution)/shard_map/pallas_call | solution.py:147
  (181 shorter events, 61.6 us)
Async XLA Ops:
  0.0 38.5 %copy-start = (bf16[256,2048]{1,0:T(8,128)(2,1)S(1)}, bf16[256,2048]{1,0:T(8,128)(2,1)}, u32[]{:S(2)}) copy-start(bf16[256,2048]{1,0:T(8,128)(2,1)} %param.15) | copy-start | bytes 3145732
  0.0 43.9 %collective-permute-start.5 = (bf16[256,1408]{1,0:T(8,128)(2,1)}, bf16[256,1408]{1,0:T(8,128)(2,1)}, u32[]{:S(2)}, u32[]{:S(2)}) collective-permute-start(bf16[256,1408]{1,0:T(8,128)(2,1)} %param.17), channel_id=1, source_target_pairs={{0,24},{4,28},{8,0},{12,4},{16,8},{20,12},{24,16},{28,20},{1,25},{... | collective-permute-start | bytes 2162696 | tf_op jit(solution)/shard_map/ppermute | solution.py:81
  5.1 56.5 %collective-permute-start.9 = (bf16[256,1408]{1,0:T(8,128)(2,1)}, bf16[256,1408]{1,0:T(8,128)(2,1)}, u32[]{:S(2)}, u32[]{:S(2)}) collective-permute-start(bf16[256,1408]{1,0:T(8,128)(2,1)} %param.17), channel_id=1, source_target_pairs={{0,4},{4,0},{8,12},{12,8},{16,20},{20,16},{24,28},{28,24},{1,5},{5... | collective-permute-start | bytes 2162696 | tf_op jit(solution)/shard_map/ppermute | solution.py:81
  6.7 61.8 %collective-permute-start.7 = (bf16[256,1408]{1,0:T(8,128)(2,1)}, bf16[256,1408]{1,0:T(8,128)(2,1)}, u32[]{:S(2)}, u32[]{:S(2)}) collective-permute-start(bf16[256,1408]{1,0:T(8,128)(2,1)} %param.17), channel_id=1, source_target_pairs={{0,8},{4,12},{8,16},{12,20},{16,24},{20,28},{24,0},{28,4},{1,9},{5... | collective-permute-start | bytes 2162696 | tf_op jit(solution)/shard_map/ppermute | solution.py:81
  8.7 16.1 %collective-permute-start = (bf16[128,256]{1,0:T(8,128)(2,1)S(1)}, bf16[128,256]{1,0:T(8,128)(2,1)S(1)}, u32[]{:S(2)}, u32[]{:S(2)}) collective-permute-start(bf16[128,256]{1,0:T(8,128)(2,1)S(1)} %slice.108), channel_id=1, source_target_pairs={{0,4},{4,8},{8,12},{12,16},{16,20},{20,24},{24,28},{1,5},{5,9},{9,... | collective-permute-start | bytes 196616 | tf_op jit(solution)/shard_map/ppermute | solution.py:16
  11.1 54.8 %collective-permute-start.18 = (bf16[256,1408]{1,0:T(8,128)(2,1)}, bf16[256,1408]{1,0:T(8,128)(2,1)}, u32[]{:S(2)}, u32[]{:S(2)}) collective-permute-start(bf16[256,1408]{1,0:T(8,128)(2,1)} %param.18), channel_id=1, source_target_pairs={{0,4},{4,0},{8,12},{12,8},{16,20},{20,16},{24,28},{28,24},{1,5},{5... | collective-permute-start | bytes 2162696 | tf_op jit(solution)/shard_map/ppermute | solution.py:81
  40.6 102.3 %collective-permute-start.1 = (bf16[512,2048]{1,0:T(8,128)(2,1)}, bf16[512,2048]{1,0:T(8,128)(2,1)S(1)}, u32[]{:S(2)}, u32[]{:S(2)}) collective-permute-start(bf16[512,2048]{1,0:T(8,128)(2,1)} %convolution_convert_fusion), channel_id=1, source_target_pairs={{0,1},{1,0},{2,3},{3,2},{4,5},{5,4},{6,7},{7,6},{8,9},{9,8},{10,11... | collective-permute-start | bytes 6291464 | tf_op jit(solution)/shard_map/ppermute | solution.py:81
  43.9 22.1 %copy-start.10 = (bf16[256,1408]{1,0:T(8,128)(2,1)S(1)}, bf16[256,1408]{1,0:T(8,128)(2,1)}, u32[]{:S(2)}) copy-start(bf16[256,1408]{1,0:T(8,128)(2,1)} %param.19) | copy-start | bytes 2162692
  43.9 24.5 %copy-start.9 = (bf16[256,1408]{1,0:T(8,128)(2,1)S(1)}, bf16[256,1408]{1,0:T(8,128)(2,1)}, u32[]{:S(2)}) copy-start(bf16[256,1408]{1,0:T(8,128)(2,1)} %param.18) | copy-start | bytes 2162692
  43.9 37.3 %collective-permute-start.14 = (bf16[256,1408]{1,0:T(8,128)(2,1)}, bf16[256,1408]{1,0:T(8,128)(2,1)}, u32[]{:S(2)}, u32[]{:S(2)}) collective-permute-start(bf16[256,1408]{1,0:T(8,128)(2,1)} %param.18), channel_id=1, source_target_pairs={{0,24},{4,28},{8,0},{12,4},{16,8},{20,12},{24,16},{28,20},{1,25},{... | collective-permute-start | bytes 2162696 | tf_op jit(solution)/shard_map/ppermute | solution.py:81
  61.6 23.4 %copy-start.20 = (bf16[1024,1408]{1,0:T(8,128)(2,1)S(1)}, bf16[1024,1408]{1,0:T(8,128)(2,1)}, u32[]{:S(2)}) copy-start(bf16[1024,1408]{1,0:T(8,128)(2,1)} %constant_dynamic-update-slice_fusion.18) | copy-start | bytes 8650756
  61.6 18.5 %collective-permute-start.29 = (bf16[256,1408]{1,0:T(8,128)(2,1)}, bf16[256,1408]{1,0:T(8,128)(2,1)S(1)}, u32[]{:S(2)}, u32[]{:S(2)}) collective-permute-start(bf16[256,1408]{1,0:T(8,128)(2,1)} %param.19), channel_id=1, source_target_pairs={{0,4},{4,0},{8,12},{12,8},{16,20},{20,16},{24,28},{28,24},{1,5},{5... | collective-permute-start | bytes 2162696 | tf_op jit(solution)/shard_map/ppermute | solution.py:81
  65.9 27.2 %collective-permute-start.23 = (bf16[256,1408]{1,0:T(8,128)(2,1)S(1)}, bf16[256,1408]{1,0:T(8,128)(2,1)}, u32[]{:S(2)}, u32[]{:S(2)}) collective-permute-start(bf16[256,1408]{1,0:T(8,128)(2,1)S(1)} %copy-done.10), channel_id=1, source_target_pairs={{0,24},{4,28},{8,0},{12,4},{16,8},{20,12},{24,16},{28,20},{1,25},{... | collective-permute-start | bytes 2162696 | tf_op jit(solution)/shard_map/ppermute | solution.py:81
  68.4 61.6 %collective-permute-start.16 = (bf16[256,1408]{1,0:T(8,128)(2,1)S(1)}, bf16[256,1408]{1,0:T(8,128)(2,1)S(1)}, u32[]{:S(2)}, u32[]{:S(2)}) collective-permute-start(bf16[256,1408]{1,0:T(8,128)(2,1)S(1)} %copy-done.9), channel_id=1, source_target_pairs={{0,8},{4,12},{8,16},{12,20},{16,24},{20,28},{24,0},{28,4},{1,9},{5... | collective-permute-start | bytes 2162696 | tf_op jit(solution)/shard_map/ppermute | solution.py:81
  80.2 49.9 %collective-permute-start.25 = (bf16[256,1408]{1,0:T(8,128)(2,1)S(1)}, bf16[256,1408]{1,0:T(8,128)(2,1)S(1)}, u32[]{:S(2)}, u32[]{:S(2)}) collective-permute-start(bf16[256,1408]{1,0:T(8,128)(2,1)S(1)} %copy-done.10), channel_id=1, source_target_pairs={{0,8},{4,12},{8,16},{12,20},{16,24},{20,28},{24,0},{28,4},{1,9},{5... | collective-permute-start | bytes 2162696 | tf_op jit(solution)/shard_map/ppermute | solution.py:81
  81.2 51.7 %collective-permute-start.6 = (bf16[128,1408]{1,0:T(8,128)(2,1)S(1)}, bf16[128,1408]{1,0:T(8,128)(2,1)S(1)}, u32[]{:S(2)}, u32[]{:S(2)}) collective-permute-start(bf16[128,1408]{1,0:T(8,128)(2,1)S(1)} %slice.114), channel_id=1, source_target_pairs={{0,24},{4,28},{8,0},{12,4},{16,8},{20,12},{24,16},{28,20},{1,25},{... | collective-permute-start | bytes 1081352 | tf_op jit(solution)/shard_map/ppermute | solution.py:81
  93.1 47.0 %collective-permute-start.8 = (bf16[128,1408]{1,0:T(8,128)(2,1)S(1)}, bf16[128,1408]{1,0:T(8,128)(2,1)S(1)}, u32[]{:S(2)}, u32[]{:S(2)}) collective-permute-start(bf16[128,1408]{1,0:T(8,128)(2,1)S(1)} %slice.115), channel_id=1, source_target_pairs={{0,8},{4,12},{8,16},{12,20},{16,24},{20,28},{24,0},{28,4},{1,9},{5... | collective-permute-start | bytes 1081352 | tf_op jit(solution)/shard_map/ppermute | solution.py:81
  130.0 35.4 %copy-start.4 = (bf16[256,1408]{1,0:T(8,128)(2,1)}, bf16[256,1408]{1,0:T(8,128)(2,1)S(1)}, u32[]{:S(2)}) copy-start(bf16[256,1408]{1,0:T(8,128)(2,1)S(1)} %collective-permute-done.16) | copy-start | bytes 2162692
  130.0 17.9 %collective-permute-start.15 = (bf16[128,1408]{1,0:T(8,128)(2,1)S(1)}, bf16[128,1408]{1,0:T(8,128)(2,1)S(1)}, u32[]{:S(2)}, u32[]{:S(2)}) collective-permute-start(bf16[128,1408]{1,0:T(8,128)(2,1)S(1)} %slice.118), channel_id=1, source_target_pairs={{0,24},{4,28},{8,0},{12,4},{16,8},{20,12},{24,16},{28,20},{1,25},{... | collective-permute-start | bytes 1081352 | tf_op jit(solution)/shard_map/ppermute | solution.py:81
  130.1 25.5 %collective-permute-start.17 = (bf16[128,1408]{1,0:T(8,128)(2,1)S(1)}, bf16[128,1408]{1,0:T(8,128)(2,1)S(1)}, u32[]{:S(2)}, u32[]{:S(2)}) collective-permute-start(bf16[128,1408]{1,0:T(8,128)(2,1)S(1)} %slice.119), channel_id=1, source_target_pairs={{0,8},{4,12},{8,16},{12,20},{16,24},{20,28},{24,0},{28,4},{1,9},{5... | collective-permute-start | bytes 1081352 | tf_op jit(solution)/shard_map/ppermute | solution.py:81
  132.9 29.5 %collective-permute-start.24 = (bf16[128,1408]{1,0:T(8,128)(2,1)S(1)}, bf16[128,1408]{1,0:T(8,128)(2,1)S(1)}, u32[]{:S(2)}, u32[]{:S(2)}) collective-permute-start(bf16[128,1408]{1,0:T(8,128)(2,1)S(1)} %slice.122), channel_id=1, source_target_pairs={{0,24},{4,28},{8,0},{12,4},{16,8},{20,12},{24,16},{28,20},{1,25},{... | collective-permute-start | bytes 1081352 | tf_op jit(solution)/shard_map/ppermute | solution.py:81
  140.1 35.9 %collective-permute-start.26 = (bf16[128,1408]{1,0:T(8,128)(2,1)}, bf16[128,1408]{1,0:T(8,128)(2,1)}, u32[]{:S(2)}, u32[]{:S(2)}) collective-permute-start(bf16[128,1408]{1,0:T(8,128)(2,1)} %slice.123), channel_id=1, source_target_pairs={{0,8},{4,12},{8,16},{12,20},{16,24},{20,28},{24,0},{28,4},{1,9},{5... | collective-permute-start | bytes 1081352 | tf_op jit(solution)/shard_map/ppermute | solution.py:81
  142.9 37.6 %collective-permute-start.10 = (bf16[256,1408]{1,0:T(8,128)(2,1)}, bf16[256,1408]{1,0:T(8,128)(2,1)}, u32[]{:S(2)}, u32[]{:S(2)}) collective-permute-start(bf16[256,1408]{1,0:T(8,128)(2,1)} %collective-permute-done.5), channel_id=1, source_target_pairs={{0,4},{4,0},{8,12},{12,8},{16,20},{20,16},{24,28},{28,24},{1,5},{5... | collective-permute-start | bytes 2162696 | tf_op jit(solution)/shard_map/ppermute | solution.py:81
  147.9 23.4 %copy-start.16 = (bf16[128,1408]{1,0:T(8,128)(2,1)}, bf16[128,1408]{1,0:T(8,128)(2,1)S(1)}, u32[]{:S(2)}) copy-start(bf16[128,1408]{1,0:T(8,128)(2,1)S(1)} %collective-permute-done.15) | copy-start | bytes 1081348
  147.9 23.4 %collective-permute-start.2 = (bf16[256,2048]{1,0:T(8,128)(2,1)S(1)}, bf16[256,2048]{1,0:T(8,128)(2,1)S(1)}, u32[]{:S(2)}, u32[]{:S(2)}) collective-permute-start(bf16[256,2048]{1,0:T(8,128)(2,1)S(1)} %slice.160), channel_id=1, source_target_pairs={{0,2},{1,3},{2,0},{3,1},{4,6},{5,7},{6,4},{7,5},{8,10},{9,11},{10,... | collective-permute-start | bytes 3145736 | tf_op jit(solution)/shard_map/ppermute | solution.py:81
  155.6 106.6 %collective-permute-start.13 = (bf16[256,1408]{1,0:T(8,128)(2,1)}, bf16[256,1408]{1,0:T(8,128)(2,1)}, u32[]{:S(2)}, u32[]{:S(2)}) collective-permute-start(bf16[256,1408]{1,0:T(8,128)(2,1)} %collective-permute-done.7), channel_id=1, source_target_pairs={{0,4},{4,0},{8,12},{12,8},{16,20},{20,16},{24,28},{28,24},{1,5},{5... | collective-permute-start | bytes 2162696 | tf_op jit(solution)/shard_map/ppermute | solution.py:81
  162.5 30.3 %collective-permute-start.19 = (bf16[256,1408]{1,0:T(8,128)(2,1)}, bf16[256,1408]{1,0:T(8,128)(2,1)}, u32[]{:S(2)}, u32[]{:S(2)}) collective-permute-start(bf16[256,1408]{1,0:T(8,128)(2,1)} %collective-permute-done.14), channel_id=1, source_target_pairs={{0,4},{4,0},{8,12},{12,8},{16,20},{20,16},{24,28},{28,24},{1,5},{5... | collective-permute-start | bytes 2162696 | tf_op jit(solution)/shard_map/ppermute | solution.py:81
  171.3 36.9 %collective-permute-start.30 = (bf16[256,1408]{1,0:T(8,128)(2,1)}, bf16[256,1408]{1,0:T(8,128)(2,1)}, u32[]{:S(2)}, u32[]{:S(2)}) collective-permute-start(bf16[256,1408]{1,0:T(8,128)(2,1)} %collective-permute-done.23), channel_id=1, source_target_pairs={{0,4},{4,0},{8,12},{12,8},{16,20},{20,16},{24,28},{28,24},{1,5},{5... | collective-permute-start | bytes 2162696 | tf_op jit(solution)/shard_map/ppermute | solution.py:81
  175.9 16.9 %copy-start.15 = (bf16[128,1408]{1,0:T(8,128)(2,1)S(1)}, bf16[128,1408]{1,0:T(8,128)(2,1)}, u32[]{:S(2)}) copy-start(bf16[128,1408]{1,0:T(8,128)(2,1)} %copy-done.14) | copy-start | bytes 1081348
  175.9 17.2 %copy-start.25 = (bf16[1024,1408]{1,0:T(8,128)(2,1)S(1)}, bf16[1024,1408]{1,0:T(8,128)(2,1)}, u32[]{:S(2)}) copy-start(bf16[1024,1408]{1,0:T(8,128)(2,1)} %constant_dynamic-update-slice_fusion.23) | copy-start | bytes 8650756
  176.0 32.2 %copy-start.17 = (bf16[128,1408]{1,0:T(8,128)(2,1)S(1)}, bf16[128,1408]{1,0:T(8,128)(2,1)}, u32[]{:S(2)}) copy-start(bf16[128,1408]{1,0:T(8,128)(2,1)} %copy-done.16) | copy-start | bytes 1081348
  176.0 36.6 %collective-permute-start.3 = (bf16[256,2048]{0,1:T(8,128)(2,1)S(1)}, bf16[256,2048]{0,1:T(8,128)(2,1)S(1)}, u32[]{:S(2)}, u32[]{:S(2)}) collective-permute-start(bf16[256,2048]{0,1:T(8,128)(2,1)S(1)} %pad_maximum_fusion.2), channel_id=1, source_target_pairs={{0,2},{1,3},{2,0},{3,1},{4,6},{5,7},{6,4},{7,5},{8,10},{9,11},{10,... | collective-permute-start | bytes 3145736 | tf_op jit(solution)/shard_map/ppermute | solution.py:81
  180.5 32.2 %copy-start.19 = (bf16[128,1408]{1,0:T(8,128)(2,1)S(1)}, bf16[128,1408]{1,0:T(8,128)(2,1)}, u32[]{:S(2)}) copy-start(bf16[128,1408]{1,0:T(8,128)(2,1)} %copy-done.18) | copy-start | bytes 1081348
  180.5 83.0 %collective-permute-start.22 = (bf16[256,1408]{1,0:T(8,128)(2,1)S(1)}, bf16[256,1408]{1,0:T(8,128)(2,1)S(1)}, u32[]{:S(2)}, u32[]{:S(2)}) collective-permute-start(bf16[256,1408]{1,0:T(8,128)(2,1)S(1)} %copy-done.5), channel_id=1, source_target_pairs={{0,4},{4,0},{8,12},{12,8},{16,20},{20,16},{24,28},{28,24},{1,5},{5... | collective-permute-start | bytes 2162696 | tf_op jit(solution)/shard_map/ppermute | solution.py:81
  192.8 38.5 %collective-permute-start.11 = (bf16[128,1408]{1,0:T(8,128)(2,1)S(1)}, bf16[128,1408]{1,0:T(8,128)(2,1)S(1)}, u32[]{:S(2)}, u32[]{:S(2)}) collective-permute-start(bf16[128,1408]{1,0:T(8,128)(2,1)S(1)} %copy-done.15), channel_id=1, source_target_pairs={{0,4},{4,0},{8,12},{12,8},{16,20},{20,16},{24,28},{28,24},{1,5},{5... | collective-permute-start | bytes 1081352 | tf_op jit(solution)/shard_map/ppermute | solution.py:81
  208.2 30.8 %collective-permute-start.20 = (bf16[128,1408]{1,0:T(8,128)(2,1)S(1)}, bf16[128,1408]{1,0:T(8,128)(2,1)S(1)}, u32[]{:S(2)}, u32[]{:S(2)}) collective-permute-start(bf16[128,1408]{1,0:T(8,128)(2,1)S(1)} %copy-done.17), channel_id=1, source_target_pairs={{0,4},{4,0},{8,12},{12,8},{16,20},{20,16},{24,28},{28,24},{1,5},{5... | collective-permute-start | bytes 1081352 | tf_op jit(solution)/shard_map/ppermute | solution.py:81
  212.6 34.6 %copy-start.26 = (bf16[1024,1408]{1,0:T(8,128)(2,1)S(1)}, bf16[1024,1408]{1,0:T(8,128)(2,1)}, u32[]{:S(2)}) copy-start(bf16[1024,1408]{1,0:T(8,128)(2,1)} %constant_dynamic-update-slice_fusion.32) | copy-start | bytes 8650756
  212.6 32.0 %collective-permute-start.31 = (bf16[128,1408]{1,0:T(8,128)(2,1)S(1)}, bf16[128,1408]{1,0:T(8,128)(2,1)S(1)}, u32[]{:S(2)}, u32[]{:S(2)}) collective-permute-start(bf16[128,1408]{1,0:T(8,128)(2,1)S(1)} %copy-done.19), channel_id=1, source_target_pairs={{0,4},{4,0},{8,12},{12,8},{16,20},{20,16},{24,28},{28,24},{1,5},{5... | collective-permute-start | bytes 1081352 | tf_op jit(solution)/shard_map/ppermute | solution.py:81
  231.3 39.9 %collective-permute-start.4 = (bf16[512,2048]{0,1:T(8,128)(2,1)S(1)}, bf16[512,2048]{0,1:T(8,128)(2,1)S(1)}, u32[]{:S(2)}, u32[]{:S(2)}) collective-permute-start(bf16[512,2048]{0,1:T(8,128)(2,1)S(1)} %pad_maximum_fusion.1), channel_id=1, source_target_pairs={{0,1},{1,0},{2,3},{3,2},{4,5},{5,4},{6,7},{7,6},{8,9},{9,8},{10,11... | collective-permute-start | bytes 6291464 | tf_op jit(solution)/shard_map/ppermute | solution.py:81
  239.0 9.3 %collective-permute-start.12 = (bf16[128,1408]{1,0:T(8,128)(2,1)S(1)}, bf16[128,1408]{1,0:T(8,128)(2,1)S(1)}, u32[]{:S(2)}, u32[]{:S(2)}) collective-permute-start(bf16[128,1408]{1,0:T(8,128)(2,1)S(1)} %slice.117), channel_id=1, source_target_pairs={{0,24},{4,28},{8,0},{12,4},{16,8},{20,12},{24,16},{28,20},{1,25},{... | collective-permute-start | bytes 1081352 | tf_op jit(solution)/shard_map/ppermute | solution.py:81
  244.7 11.4 %collective-permute-start.21 = (bf16[128,1408]{1,0:T(8,128)(2,1)S(1)}, bf16[128,1408]{1,0:T(8,128)(2,1)S(1)}, u32[]{:S(2)}, u32[]{:S(2)}) collective-permute-start(bf16[128,1408]{1,0:T(8,128)(2,1)S(1)} %slice.120), channel_id=1, source_target_pairs={{0,24},{4,28},{8,0},{12,4},{16,8},{20,12},{24,16},{28,20},{1,25},{... | collective-permute-start | bytes 1081352 | tf_op jit(solution)/shard_map/ppermute | solution.py:81
  248.3 13.9 %collective-permute-start.32 = (bf16[128,1408]{1,0:T(8,128)(2,1)S(1)}, bf16[128,1408]{1,0:T(8,128)(2,1)S(1)}, u32[]{:S(2)}, u32[]{:S(2)}) collective-permute-start(bf16[128,1408]{1,0:T(8,128)(2,1)S(1)} %slice.127), channel_id=1, source_target_pairs={{0,24},{4,28},{8,0},{12,4},{16,8},{20,12},{24,16},{28,20},{1,25},{... | collective-permute-start | bytes 1081352 | tf_op jit(solution)/shard_map/ppermute | solution.py:81
  256.0 15.0 %collective-permute-start.33 = (bf16[256,1408]{1,0:T(8,128)(2,1)S(1)}, bf16[256,1408]{1,0:T(8,128)(2,1)S(1)}, u32[]{:S(2)}, u32[]{:S(2)}) collective-permute-start(bf16[256,1408]{1,0:T(8,128)(2,1)S(1)} %copy-done.7), channel_id=1, source_target_pairs={{0,4},{4,0},{8,12},{12,8},{16,20},{20,16},{24,28},{28,24},{1,5},{5... | collective-permute-start | bytes 2162696 | tf_op jit(solution)/shard_map/ppermute | solution.py:81
  299.7 6.1 %collective-permute-start.34 = (bf16[512,1024]{1,0:T(8,128)(2,1)S(1)}, bf16[512,1024]{1,0:T(8,128)(2,1)S(1)}, u32[]{:S(2)}, u32[]{:S(2)}) collective-permute-start(bf16[512,1024]{1,0:T(8,128)(2,1)S(1)} %convolution_convert_fusion.2), channel_id=1, source_target_pairs={{0,1},{1,0},{2,3},{3,2},{4,5},{5,4},{6,7},{7,6},{8,9},{9,8},{10,11... | collective-permute-start | bytes 3145736 | tf_op jit(solution)/shard_map/ppermute | solution.py:81
  301.6 6.3 %collective-permute-start.27 = (bf16[512,1024]{1,0:T(8,128)(2,1)S(1)}, bf16[512,1024]{1,0:T(8,128)(2,1)S(1)}, u32[]{:S(2)}, u32[]{:S(2)}) collective-permute-start(bf16[512,1024]{1,0:T(8,128)(2,1)S(1)} %convolution_convert_fusion.4), channel_id=1, source_target_pairs={{0,1},{1,0},{2,3},{3,2},{4,5},{5,4},{6,7},{7,6},{8,9},{9,8},{10,11... | collective-permute-start | bytes 3145736 | tf_op jit(solution)/shard_map/ppermute | solution.py:81
  306.3 14.9 %collective-permute-start.35 = (bf16[256,1024]{1,0:T(8,128)(2,1)S(1)}, bf16[256,1024]{1,0:T(8,128)(2,1)S(1)}, u32[]{:S(2)}, u32[]{:S(2)}) collective-permute-start(bf16[256,1024]{1,0:T(8,128)(2,1)S(1)} %slice.161), channel_id=1, source_target_pairs={{0,2},{1,3},{2,0},{3,1},{4,6},{5,7},{6,4},{7,5},{8,10},{9,11},{10,... | collective-permute-start | bytes 1572872 | tf_op jit(solution)/shard_map/ppermute | solution.py:81
  308.3 23.1 %collective-permute-start.28 = (bf16[256,1024]{1,0:T(8,128)(2,1)S(1)}, bf16[256,1024]{1,0:T(8,128)(2,1)S(1)}, u32[]{:S(2)}, u32[]{:S(2)}) collective-permute-start(bf16[256,1024]{1,0:T(8,128)(2,1)S(1)} %slice.162), channel_id=1, source_target_pairs={{0,2},{1,3},{2,0},{3,1},{4,6},{5,7},{6,4},{7,5},{8,10},{9,11},{10,... | collective-permute-start | bytes 1572872 | tf_op jit(solution)/shard_map/ppermute | solution.py:81
  310.6 28.6 %copy-start.1 = (bf16[256,2048]{1,0:T(8,128)(2,1)S(1)}, bf16[256,2048]{1,0:T(8,128)(2,1)}, u32[]{:S(2)}) copy-start(bf16[256,2048]{1,0:T(8,128)(2,1)} %param.15) | copy-start | bytes 3145732
  (19 other events, 131.2 us)
